TPU v7x, 32 devices: a whole 2x2x4 slice. The times are simulated.
32 devices in a mesh: ep: 8 (over z, y), tp: 4 (over x, core).
Axes of the slice: x: 2, y: 2, z: 4, core: 2. Of those that a mesh axis runs over, the one named last changes fastest.
Arguments:
- hidden: bfloat16 [32, 2048], P('ep'), may hold values from -6 to 6
- lengths: int32 [32], P(('ep', 'tp')), may hold values from 1 to 1535, 24576 in all
- latent_cache: bfloat16 [32, 1536, 512], P(('ep', 'tp')), may hold values from -6 to 6
- cache_rotary: bfloat16 [32, 32, 1536], P(('ep', 'tp')), may hold values from -1500 to 1500
- attn_gain: bfloat16 [2048], replicated, may hold values from 0.099609375 to 1.8984375
- w_query_nope: bfloat16 [2048, 1024], P(None, 'tp'), may hold values from -0.125 to 0.125
- w_query_rope: bfloat16 [2048, 512], P(None, 'tp'), may hold values from -0.125 to 0.125
- latent_weight: bfloat16 [2048, 512], replicated, may hold values from -0.125 to 0.125
- w_rotary_key: bfloat16 [2048, 32], replicated, may hold values from -0.125 to 0.125
- latent_norm_gain: bfloat16 [512], replicated, may hold values from 0.099609375 to 1.8984375
- key_up_weight: bfloat16 [1024, 512], P('tp'), may hold values from -0.75 to 0.75
- value_up_weight: bfloat16 [512, 1024], P(None, 'tp'), may hold values from -0.25 to 0.25
- head_gain: bfloat16 [1024], P('tp'), may hold values from 0.099609375 to 1.8984375
- w_output: bfloat16 [1024, 2048], P('tp'), may hold values from -0.1875 to 0.1875
- ffn_gain: bfloat16 [2048], replicated, may hold values from 0.099609375 to 1.8984375
- expert_ids: int32 [32, 4], P('ep'), may hold values from 0 to 7, all different within a row; in each aligned block of 4 rows (0 to 3, 4 to 7, ...) at most 3 rows name the same one
- expert_weights: float32 [32, 4], P('ep'), may hold values from 0.2 to 1.2
- w_expert_gate: bfloat16 [8, 2048, 2048], P('ep', None, 'tp'), may hold values from -0.125 to 0.125
- w_expert_up: bfloat16 [8, 2048, 2048], P('ep', None, 'tp'), may hold values from -0.125 to 0.125
- w_expert_down: bfloat16 [8, 2048, 2048], P('ep', 'tp'), may hold values from -0.125 to 0.125
- w_shared_gate: bfloat16 [2048, 1024], P(None, 'tp'), may hold values from -0.125 to 0.125
- w_shared_up: bfloat16 [2048, 1024], P(None, 'tp'), may hold values from -0.125 to 0.125
- w_shared_down: bfloat16 [1024, 2048], P('tp'), may hold values from -0.1875 to 0.1875
- w_dense_up: bfloat16 [2048, 2048], P(None, 'tp'), may hold values from -0.125 to 0.125
- w_dense_down: bfloat16 [2048, 2048], P('tp'), may hold values from -0.125 to 0.125
- dense_gate: bfloat16 [2048], replicated, may hold values from -0.125 to 0.125
Outputs:
- layer_out: bfloat16 [32, 2048], P('ep', 'tp')
Inputs may be any that keep to these rules, and one draw needn't show every extreme that they name: `lengths`: past positions of each sequence; the longest has exactly 1535, so every cache has room for the new token. `expert_ids`: A row's 4 experts differ. Among the rows of one index of ep (4 rows), no expert is named by more than 3 of them, a bound that some block reaches.
All inputs are finite; a program needn't handle non-finite values. No bound on the sum of `lengths` on one device may be relied on, other than what follows from the above.
Results may differ from a plain program's by a relative error of at most 0.024.
Values may be sent and summed in bfloat16 or wider, within the bound.
A program may use at most 64 MiB of HBM per device.

v0:
```python
import functools
import math
from typing import Any, NamedTuple

import jax
import jax.numpy as jnp
import numpy as np
from jax import lax
from jax.experimental import pallas as pl
from jax.experimental.pallas import tpu as pltpu
from jax.sharding import PartitionSpec as P

PLAIN_QUERY = 64
ROPE = 32
EPS = 1e-06
F32 = jnp.float32
BF16 = jnp.bfloat16
MESH = pl.DeviceIdType.MESH
VMEM = pltpu.VMEM

class Arrays(NamedTuple):
    hidden: Any
    attn_gain: Any
    w_query_nope: Any
    w_query_rope: Any
    key_up_weight: Any
    latent_norm_gain: Any
    w_rotary_key: Any
    latent_weight: Any
    cache_rotary: Any
    latent_cache: Any
    value_up_weight: Any
    head_gain: Any
    w_output: Any
    ffn_gain: Any
    dense_gate: Any
    expert_ids: Any
    expert_weights: Any
    w_shared_gate: Any
    w_shared_up: Any
    w_dense_up: Any
    w_shared_down: Any
    w_dense_down: Any
    w_expert_gate: Any
    w_expert_up: Any
    w_expert_down: Any


def dot(a, b):
    return jnp.dot(a, b, preferred_element_type=F32)


def dot_t(a, b):
    return lax.dot_general(a, b, (((1,), (1,)), ((), ())), preferred_element_type=F32)


def as_row(ref):
    return ref[...].astype(F32).reshape(1, -1)


def norm_factor(values):
    return lax.rsqrt(jnp.mean(values * values, axis=-1, keepdims=True) + EPS)


def rounded(values):
    return values.astype(BF16).astype(F32)


def stack(ref, count):
    return jnp.concatenate([ref[i].astype(F32) for i in range(count)], axis=0)


def far_first(count):
    return sorted(range(1, count), key=lambda d: -min(d, count - d))


def iota(shape, dim):
    return lax.broadcasted_iota(jnp.int32, shape, dim)


def half_turn(values):
    half = values.shape[-1] // 2
    return jnp.concatenate([values[:, half:], values[:, :half]], axis=1)


def layer_kernel(n_ep, n_tp, *refs):
    count = len(Arrays._fields)
    lengths_hbm = refs[0]
    hbm = refs[1 : 1 + count]
    out_ref = refs[1 + count]
    vm = refs[2 + count : 2 + 2 * count]
    (
        lengths_ref,
        fetch_sem,
        q_send,
        q_recv,
        a_send,
        a_recv,
        p_buf,
        mid_buf,
        x_buf,
        s_send,
        s_recv,
        e_send,
        e_recv,
        r_send,
        r_recv,
        tp_sems,
        ep_sems,
    ) = refs[2 + 2 * count :]
    ep = lax.axis_index("ep")
    tp = lax.axis_index("tp")

    fetches = [
        pltpu.make_async_copy(source, target, fetch_sem.at[i])
        for i, (source, target) in enumerate(zip(hbm, vm))
    ]
    place = Arrays(*range(count))
    fetch_lengths = pltpu.make_async_copy(lengths_hbm, lengths_ref, fetch_sem.at[count])

    def begin(first, last):
        for fetch in fetches[first : last + 1]:
            fetch.start()

    begin(place.hidden, place.key_up_weight)
    fetch_lengths.start()

    def loader(fetch, ref):
        def load():
            fetch.wait()
            return ref

        return load

    load = Arrays(*map(loader, fetches, vm))

    def tp_peer(d):
        return lax.rem(tp + d, n_tp)

    def ep_peer(d):
        return lax.rem(ep + d, n_ep)

    barrier = pltpu.get_barrier_semaphore()
    for d in range(1, n_tp):
        pl.semaphore_signal(barrier, inc=1, device_id=(ep, tp_peer(d)), device_id_type=MESH)
    for d in range(1, n_ep):
        pl.semaphore_signal(barrier, inc=1, device_id=(ep_peer(d), tp), device_id_type=MESH)

    def tp_copy(phase, d, src, dst, to):
        return pltpu.make_async_remote_copy(
            src_ref=src,
            dst_ref=dst,
            send_sem=tp_sems.at[phase, 0, d],
            recv_sem=tp_sems.at[phase, 1, d],
            device_id=(ep, to),
            device_id_type=MESH,
        )

    def ep_copy(phase, d, src, dst, to):
        return pltpu.make_async_remote_copy(
            src_ref=src,
            dst_ref=dst,
            send_sem=ep_sems.at[phase, 0, d],
            recv_sem=ep_sems.at[phase, 1, d],
            device_id=(to, tp),
            device_id_type=MESH,
        )

    started = []

    def go(copy):
        copy.start()
        started.append(copy)
        return copy

    hidden = load.hidden()[...].astype(F32)
    rows, width = hidden.shape
    gain = as_row(load.attn_gain())
    normed = (hidden * norm_factor(hidden) * gain).astype(BF16)
    w_query_nope = load.w_query_nope()
    w_query_rope = load.w_query_rope()
    begin(place.latent_norm_gain, place.latent_cache)
    q_nope = rounded(dot(normed, w_query_nope[...]))
    q_rope = rounded(dot(normed, w_query_rope[...]))
    heads = q_nope.shape[1] // PLAIN_QUERY
    latent = Arrays(*vm).latent_cache.shape[1]

    def by_head(values, unit):
        wide = jnp.concatenate(
            [jnp.broadcast_to(values[i : i + 1], (heads, values.shape[1])) for i in range(rows)],
            axis=0,
        )
        head = iota(wide.shape, 0) % heads
        return jnp.where(iota(wide.shape, 1) // unit == head, wide, 0.0).astype(BF16)

    q_latent = dot(by_head(q_nope, PLAIN_QUERY), load.key_up_weight()[...])
    rope_cols = q_rope.shape[1]
    pick = (iota((rope_cols, ROPE), 0) % ROPE == iota((rope_cols, ROPE), 1)).astype(F32)
    q_rot = dot(by_head(q_rope, ROPE), pick.astype(BF16))
    for i in range(rows):
        part = slice(i * heads, (i + 1) * heads)
        q_send[i, :, :latent] = q_latent[part].astype(q_send.dtype)
        q_send[i, :, latent : latent + ROPE] = q_rot[part].astype(q_send.dtype)
    pl.semaphore_wait(barrier, n_tp + n_ep - 2)
    for d in far_first(n_tp):
        go(tp_copy(0, d, q_send.at[tp_peer(d)], q_recv.at[tp], tp_peer(d)))
    q_recv[tp] = q_send[tp]

    own = iota((rows, 1), 0) == tp
    raw_key = dot_t(normed, load.w_rotary_key()[...])
    raw_key = jnp.sum(jnp.where(own, raw_key, 0.0), axis=0, keepdims=True)
    raw_latent = dot(normed, load.latent_weight()[...])
    raw_latent = jnp.sum(jnp.where(own, raw_latent, 0.0), axis=0, keepdims=True)
    latent_gain = as_row(load.latent_norm_gain())
    new_latent = rounded(raw_latent * norm_factor(raw_latent) * latent_gain)
    fetch_lengths.wait()
    length = lengths_ref[...].reshape(1, 1)
    unit = iota((1, ROPE), 1)
    half = ROPE // 2
    inverse = jnp.zeros((1, ROPE), F32)
    for j in range(half):
        inverse = jnp.where(unit % half == j, np.float32(10000.0 ** (-j / half)).item(), inverse)
    angles = length.astype(F32) * inverse
    cosines = jnp.cos(angles)
    sines = jnp.where(unit < half, -1.0, 1.0) * jnp.sin(angles)
    new_key = rounded(raw_key * cosines + half_turn(raw_key) * sines)
    rotary = load.cache_rotary()[...]
    cache_ref = load.latent_cache()
    begin(place.value_up_weight, place.w_expert_down)

    for d in range(1, n_tp):
        started[d - 1].wait_recv()
    query = stack(q_recv, n_tp)
    q_lat = query[:, :latent]
    v = query[:, latent : latent + ROPE]
    q_rotated = rounded(v * cosines + half_turn(v) * sines)
    scale = (PLAIN_QUERY + ROPE) ** (-0.5)
    scores = dot_t(q_lat.astype(BF16), cache_ref[...])
    scores = scores + dot(q_rotated.astype(BF16), rotary)
    scores = jnp.where(iota(scores.shape, 1) < length, scores * scale, -jnp.inf)
    own_score = jnp.sum(q_lat * new_latent, axis=1, keepdims=True)
    own_score = (own_score + jnp.sum(q_rotated * new_key, axis=1, keepdims=True)) * scale
    peak = jnp.maximum(jnp.max(scores, axis=1, keepdims=True), own_score)
    exps = jnp.exp(scores - peak)
    own_exp = jnp.exp(own_score - peak)
    total = jnp.sum(exps, axis=1, keepdims=True) + own_exp
    probs = (exps / total).astype(BF16)
    own_prob = rounded(own_exp / total)
    attended = dot(probs, cache_ref[...]) + own_prob * new_latent
    for t in range(n_tp):
        a_send[t] = attended[t * heads : (t + 1) * heads].astype(a_send.dtype)
    back = [
        go(tp_copy(1, d, a_send.at[tp_peer(d)], a_recv.at[tp], tp_peer(d))) for d in far_first(n_tp)
    ]
    a_recv[tp] = a_send[tp]

    value_up = load.value_up_weight()[...]
    head_gain = as_row(load.head_gain())
    w_output = load.w_output()
    for copy in back:
        copy.wait_recv()
    values = dot(stack(a_recv, n_tp).astype(BF16), value_up)
    value_units = values.shape[1] // heads
    mine = iota(values.shape, 1) // value_units == iota(values.shape, 0) % heads
    values = jnp.where(mine, values, 0.0)
    mean = jnp.sum(values * values, axis=1, keepdims=True) / value_units
    values = values * lax.rsqrt(mean + EPS)
    values = jnp.concatenate(
        [
            jnp.sum(values[i * heads : (i + 1) * heads], axis=0, keepdims=True)
            for i in range(rows)
        ],
        axis=0,
    )
    head_out = (values * head_gain).astype(BF16)
    p_buf[tp] = dot(head_out, w_output[...]).astype(BF16)
    shares = [go(tp_copy(2, d, p_buf.at[tp], p_buf.at[tp], tp_peer(d))) for d in far_first(n_tp)]
    ffn_gain = as_row(load.ffn_gain())
    gate_vector = as_row(load.dense_gate())
    for copy in shares:
        copy.wait_recv()
    attention = p_buf[0].astype(F32)
    for t in range(1, n_tp):
        attention = attention + p_buf[t].astype(F32)
    middle = rounded(hidden + attention)
    cols = width // n_tp
    normed_ffn = (middle * norm_factor(middle) * ffn_gain).astype(BF16)
    x_buf[ep] = normed_ffn
    gathers = [go(ep_copy(0, d, x_buf.at[ep], x_buf.at[ep], ep_peer(d))) for d in far_first(n_ep)]

    for t in range(n_tp):
        mid_buf[t] = middle[:, t * cols : (t + 1) * cols]
    gate_pre = dot(normed_ffn, load.w_shared_gate()[...])
    up_pre = dot(normed_ffn, load.w_shared_up()[...])
    shared_act = (gate_pre / (1.0 + jnp.exp(-gate_pre)) * up_pre).astype(BF16)
    pre = dot(normed_ffn, load.w_dense_up()[...])
    inner = math.sqrt(2.0 / math.pi) * (pre + 0.044715 * (pre * pre * pre))
    dense_act = (0.5 * pre * (1.0 + jnp.tanh(inner))).astype(BF16)
    mix = jnp.sum(normed_ffn.astype(F32) * gate_vector, axis=1, keepdims=True)
    mix = 1.0 / (1.0 + jnp.exp(-mix))
    side = dot(shared_act, load.w_shared_down()[...])
    side = side + mix * dot(dense_act, load.w_dense_down()[...])
    for t in range(n_tp):
        s_send[t] = side[:, t * cols : (t + 1) * cols].astype(BF16)
    sides = [
        go(tp_copy(3, d, s_send.at[tp_peer(d)], s_recv.at[tp], tp_peer(d))) for d in far_first(n_tp)
    ]
    s_recv[tp] = s_send[tp]

    w_gate = load.w_expert_gate()
    w_up = load.w_expert_up()
    w_down = load.w_expert_down()
    for copy in gathers:
        copy.wait_recv()
    arrived = stack(x_buf, n_ep).astype(BF16)
    gate_pre = dot(arrived, w_gate[0])
    up_pre = dot(arrived, w_up[0])
    act = (gate_pre / (1.0 + jnp.exp(-gate_pre)) * up_pre).astype(BF16)
    def down(t):
        at = pl.ds(pl.multiple_of(t * cols, cols), cols)
        return dot(act, w_down[0, :, at]).astype(BF16)

    parts = []
    for d in far_first(n_tp):
        to = tp_peer(d)
        e_send[to] = down(to)
        parts.append(go(tp_copy(4, d, e_send.at[to], e_recv.at[tp], to)))
    e_recv[tp] = down(tp)
    for copy in sides:
        copy.wait_recv()
    result = mid_buf[tp]
    for t in range(n_tp):
        result = result + s_recv[t].astype(F32)
    ids = load.expert_ids()[...]
    weights = load.expert_weights()[...]
    for copy in parts:
        copy.wait_recv()
    summed = e_recv[0].astype(F32)
    for t in range(1, n_tp):
        summed = summed + e_recv[t].astype(F32)
    for g in range(n_ep):
        r_send[g] = summed[g * rows : (g + 1) * rows].astype(BF16)
    returns = [
        go(ep_copy(1, d, r_send.at[ep_peer(d)], r_recv.at[ep], ep_peer(d))) for d in far_first(n_ep)
    ]
    r_recv[ep] = r_send[ep]
    for copy in returns:
        copy.wait_recv()
    for e in range(n_ep):
        weight = jnp.sum(jnp.where(ids == e, weights, 0.0), axis=1, keepdims=True)
        result = result + weight * r_recv[e].astype(F32)
    out_ref[...] = result.astype(BF16)
    for copy in started:
        copy.wait_send()


def on_device(
    n_ep,
    n_tp,
    hidden,
    lengths,
    latent_cache,
    cache_rotary,
    attn_gain,
    w_query_nope,
    w_query_rope,
    latent_weight,
    w_rotary_key,
    latent_norm_gain,
    key_up_weight,
    value_up_weight,
    head_gain,
    w_output,
    ffn_gain,
    expert_ids,
    expert_weights,
    w_expert_gate,
    w_expert_up,
    w_expert_down,
    w_shared_gate,
    w_shared_up,
    w_shared_down,
    w_dense_up,
    w_dense_down,
    dense_gate,
):
    arrays = Arrays(
        hidden=hidden,
        attn_gain=attn_gain,
        w_query_nope=w_query_nope,
        w_query_rope=w_query_rope,
        key_up_weight=key_up_weight,
        latent_norm_gain=latent_norm_gain,
        w_rotary_key=w_rotary_key.T,
        latent_weight=latent_weight,
        cache_rotary=cache_rotary.reshape(cache_rotary.shape[1:]),
        latent_cache=latent_cache.reshape(latent_cache.shape[1:]),
        value_up_weight=value_up_weight,
        head_gain=head_gain,
        w_output=w_output,
        ffn_gain=ffn_gain,
        dense_gate=dense_gate,
        expert_ids=expert_ids,
        expert_weights=expert_weights,
        w_shared_gate=w_shared_gate,
        w_shared_up=w_shared_up,
        w_dense_up=w_dense_up,
        w_shared_down=w_shared_down,
        w_dense_down=w_dense_down,
        w_expert_gate=w_expert_gate,
        w_expert_up=w_expert_up,
        w_expert_down=w_expert_down,
    )
    rows, width = hidden.shape
    heads = w_query_nope.shape[1] // PLAIN_QUERY
    latent = latent_cache.shape[2]
    cols = width // n_tp
    message = latent + 128
    any_space = pl.BlockSpec(memory_space=pltpu.HBM)
    return pl.pallas_call(
        functools.partial(layer_kernel, n_ep, n_tp),
        out_shape=jax.ShapeDtypeStruct((rows, cols), BF16),
        in_specs=[any_space] * (1 + len(arrays)),
        out_specs=pl.BlockSpec(memory_space=pltpu.VMEM),
        scratch_shapes=[VMEM(a.shape, a.dtype) for a in arrays]
        + [
            VMEM(lengths.shape, lengths.dtype),
            pltpu.SemaphoreType.DMA((len(arrays) + 1,)),
            VMEM((rows, heads, message), BF16),
            VMEM((n_tp, heads, message), BF16),
            VMEM((n_tp, heads, latent), BF16),
            VMEM((n_tp, heads, latent), BF16),
            VMEM((n_tp, rows, width), BF16),
            VMEM((n_tp, rows, cols), F32),
            VMEM((n_ep, rows, width), BF16),
            VMEM((n_tp, rows, cols), BF16),
            VMEM((n_tp, rows, cols), BF16),
            VMEM((n_tp, n_ep * rows, cols), BF16),
            VMEM((n_tp, n_ep * rows, cols), BF16),
            VMEM((n_ep, rows, cols), BF16),
            VMEM((n_ep, rows, cols), BF16),
            pltpu.SemaphoreType.DMA((5, 2, n_tp)),
            pltpu.SemaphoreType.DMA((2, 2, n_ep)),
        ],
        compiler_params=pltpu.CompilerParams(
            collective_id=0, has_side_effects=True, vmem_limit_bytes=60 * 1024 * 1024
        ),
    )(lengths, *arrays)


def solution(mesh):
    placed = (
        P("ep", None),
        P(("ep", "tp")),
        P(("ep", "tp"), None, None),
        P(("ep", "tp"), None, None),
        P(),
        P(None, "tp"),
        P(None, "tp"),
        P(),
        P(),
        P(),
        P("tp", None),
        P(None, "tp"),
        P("tp"),
        P("tp", None),
        P(),
        P("ep", None),
        P("ep", None),
        P("ep", None, "tp"),
        P("ep", None, "tp"),
        P("ep", "tp", None),
        P(None, "tp"),
        P(None, "tp"),
        P("tp", None),
        P(None, "tp"),
        P("tp", None),
        P(),
    )
    step = functools.partial(on_device, mesh.shape["ep"], mesh.shape["tp"])
    return jax.shard_map(
        step, mesh=mesh, in_specs=placed, out_specs=P("ep", "tp"), check_vma=False
    )
```

profile of v0, /device:TPU:0, one launch (start us, length us, event | category | flops | bytes accessed | tf_op | source)
XLA Modules:
  0.0 33.3 jit_solution(16461492365439852503)
XLA Ops:
  0.7 31.4 %shard_map.244 = bf16[4,512]{1,0:T(4,128)(2,1)} custom-call(s32[1]{0:T(128)S(6)} %copy.28.refs_0_, bf16[4,2048]{1,0:T(4,128)(2,1)} %refs_1_.1, bf16[2048]{0:T(1024)(128)(2,1)} %refs_2_.1, bf16[2048,256]{1,0:T(8,128)(2,1)} %refs_3_.1, bf16[2048,128]{1,0:T(8,128)(2,1)} %refs_4_.1, bf16[256,512]{1,0:T(8,128)(2,1)} %refs_5_.1, bf16[512]{0:T(512)(128)(2,1)} %refs_6_.1, ...), custom_call_target="tpu_custom_call" | custom-call | tf_op jit(solution)/shard_map/pallas_call | solution.py:420
  32.0 1.3 %copy.29 = bf16[4,512]{1,0:T(4,128)(2,1)} copy(bf16[4,512]{1,0:T(4,128)(2,1)} %shard_map.244) | data formatting | bytes 8192
where the time goes:
time: 33.6 us; the launch traced here: 33.3 us
  Pallas kernels  31.4 us (93%)
  local copies, waits for them, and re-layouts  1.28 us (4%)
  between operations  0.66 us (2%)
    pallas_call x1, Pallas kernels, on_device(): pl.pallas_call(functools.partial(layer_kernel, n_ep, n_tp), out_shape=jax...  31.4 us
    unnamed x1, local copies, waits for them, and re-layouts  1.28 us

commit v1 on v0

--- a/solution.py
+++ b/solution.py
@@ -74,6 +74,10 @@
     return sorted(range(1, count), key=lambda d: -min(d, count - d))
 
 
+def meet_rounds(count):
+    return max(2, (count - 2).bit_length())
+
+
 def iota(shape, dim):
     return lax.broadcasted_iota(jnp.int32, shape, dim)
 
@@ -107,6 +111,7 @@
         r_recv,
         tp_sems,
         ep_sems,
+        meet_sems,
     ) = refs[2 + 2 * count :]
     ep = lax.axis_index("ep")
     tp = lax.axis_index("tp")
@@ -143,8 +148,29 @@
     barrier = pltpu.get_barrier_semaphore()
     for d in range(1, n_tp):
         pl.semaphore_signal(barrier, inc=1, device_id=(ep, tp_peer(d)), device_id_type=MESH)
-    for d in range(1, n_ep):
-        pl.semaphore_signal(barrier, inc=1, device_id=(ep_peer(d), tp), device_id_type=MESH)
+
+    def greet(semaphores, reach):
+        for side, step in enumerate((reach, -reach)):
+
+            @pl.when((ep + step >= 0) & (ep + step < n_ep))
+            def _():
+                pl.semaphore_signal(
+                    semaphores[side], inc=1, device_id=(ep + step, tp), device_id_type=MESH
+                )
+
+    def greeted(semaphores, reach):
+        for side, step in enumerate((-reach, reach)):
+
+            @pl.when((ep + step >= 0) & (ep + step < n_ep))
+            def _():
+                pl.semaphore_wait(semaphores[side], 1)
+
+    reaches = [2**r for r in range(meet_rounds(n_ep))]
+
+    def meet(r):
+        return [meet_sems.at[r % len(reaches), side] for side in range(2)]
+
+    greet([barrier, barrier], 1)
 
     def tp_copy(phase, d, src, dst, to):
         return pltpu.make_async_remote_copy(
@@ -201,7 +227,9 @@
         part = slice(i * heads, (i + 1) * heads)
         q_send[i, :, :latent] = q_latent[part].astype(q_send.dtype)
         q_send[i, :, latent : latent + ROPE] = q_rot[part].astype(q_send.dtype)
-    pl.semaphore_wait(barrier, n_tp + n_ep - 2)
+    beside = jnp.where(ep > 0, 1, 0) + jnp.where(ep < n_ep - 1, 1, 0)
+    pl.semaphore_wait(barrier, n_tp - 1 + beside)
+    greet(meet(0), reaches[0])
     for d in far_first(n_tp):
         go(tp_copy(0, d, q_send.at[tp_peer(d)], q_recv.at[tp], tp_peer(d)))
     q_recv[tp] = q_send[tp]
@@ -228,6 +256,8 @@
     cache_ref = load.latent_cache()
     begin(place.value_up_weight, place.w_expert_down)
 
+    greeted(meet(0), reaches[0])
+    greet(meet(1), reaches[1])
     for d in range(1, n_tp):
         started[d - 1].wait_recv()
     query = stack(q_recv, n_tp)
@@ -257,6 +287,9 @@
     value_up = load.value_up_weight()[...]
     head_gain = as_row(load.head_gain())
     w_output = load.w_output()
+    for r in range(1, len(reaches) - 1):
+        greeted(meet(r), reaches[r])
+        greet(meet(r + 1), reaches[r + 1])
     for copy in back:
         copy.wait_recv()
     values = dot(stack(a_recv, n_tp).astype(BF16), value_up)
@@ -277,6 +310,7 @@
     shares = [go(tp_copy(2, d, p_buf.at[tp], p_buf.at[tp], tp_peer(d))) for d in far_first(n_tp)]
     ffn_gain = as_row(load.ffn_gain())
     gate_vector = as_row(load.dense_gate())
+    greeted(meet(-1), reaches[-1])
     for copy in shares:
         copy.wait_recv()
     attention = p_buf[0].astype(F32)
@@ -419,7 +453,7 @@
     any_space = pl.BlockSpec(memory_space=pltpu.HBM)
     return pl.pallas_call(
         functools.partial(layer_kernel, n_ep, n_tp),
-        out_shape=jax.ShapeDtypeStruct((rows, cols), BF16),
+        out_shape=pltpu.VMEM((rows, cols), BF16),
         in_specs=[any_space] * (1 + len(arrays)),
         out_specs=pl.BlockSpec(memory_space=pltpu.VMEM),
         scratch_shapes=[VMEM(a.shape, a.dtype) for a in arrays]
@@ -441,6 +475,7 @@
             VMEM((n_ep, rows, cols), BF16),
             pltpu.SemaphoreType.DMA((5, 2, n_tp)),
             pltpu.SemaphoreType.DMA((2, 2, n_ep)),
+            pltpu.SemaphoreType.REGULAR((meet_rounds(n_ep), 2)),
         ],
         compiler_params=pltpu.CompilerParams(
             collective_id=0, has_side_effects=True, vmem_limit_bytes=60 * 1024 * 1024

time: 33.6 us -> 30 us (0.89)
  Pallas kernels: 31.4 us -> 28.5 us
  local copies, waits for them, and re-layouts: 1.28 us -> 0.6 us
    pallas_call x1, Pallas kernels: 31.4 us -> 28.5 us  [on_device(): pl.pallas_call(functools.partial(layer_kernel, n_ep, n_tp), out_shape=plt...]
    unnamed x1, local copies, waits for them, and re-layouts: 1.28 us -> 0.6 us
where the time goes in v1:
time: 30 us; the launch traced here: 29.8 us
  Pallas kernels  28.5 us (95%)
  between operations  0.66 us (2%)
  local copies, waits for them, and re-layouts  0.6 us (2%)
    pallas_call x1, Pallas kernels, on_device(): pl.pallas_call(functools.partial(layer_kernel, n_ep, n_tp), out_shape=plt...  28.5 us

profile of v1, /device:TPU:0, one launch (start us, length us, event | category | flops | bytes accessed | tf_op | source)
XLA Modules:
  0.0 29.8 jit_solution(15976694595856724455)
XLA Ops:
  0.7 28.5 %shard_map.244 = bf16[4,512]{1,0:T(4,128)(2,1)S(1)} custom-call(s32[1]{0:T(128)S(6)} %copy.29.refs_0_, bf16[4,2048]{1,0:T(4,128)(2,1)} %refs_1_.1, bf16[2048]{0:T(1024)(128)(2,1)} %refs_2_.1, bf16[2048,256]{1,0:T(8,128)(2,1)} %refs_3_.1, bf16[2048,128]{1,0:T(8,128)(2,1)} %refs_4_.1, bf16[256,512]{1,0:T(8,128)(2,1)} %refs_5_.1, bf16[512]{0:T(512)(128)(2,1)} %refs_6_.1, ...), custom_call_target="tpu_custom_call" | custom-call | tf_op jit(solution)/shard_map/pallas_call | solution.py:454
  29.2 0.6 %copy.28 = bf16[4,512]{1,0:T(4,128)(2,1)} copy(bf16[4,512]{1,0:T(4,128)(2,1)S(1)} %shard_map.244) | data formatting | bytes 8192
